TPU v7x, 32 devices: a whole 2x2x4 slice. The times are simulated.
32 devices in a mesh: gr: 2 (over core), sp: 8 (over z, y), tp: 2 (over x).
Axes of the slice: x: 2, y: 2, z: 4, core: 2. Of those that a mesh axis runs over, the one named last changes fastest.
Arguments:
- mixer_input: bfloat16 [16, 1536, 2048], P(('gr', 'tp'), 'sp'), may hold values from -16.8 to 16.8
- key_weight: bfloat16 [2048, 256], P('tp'), may hold values from -0.125 to 0.125
- content_projection_matrix: bfloat16 [2048, 256], P('tp'), may hold values from -0.125 to 0.125
- new_queries: bfloat16 [16, 32, 64], P(('gr', 'sp'), 'tp'), may hold values from -6 to 6
- head_stick_offset: float32 [32], replicated, may hold values from -11 to -4
Outputs:
- kv_cache: bfloat16 [16, 4, 1536, 128], P(('gr', 'sp'), 'tp')
- initial_attended_output: bfloat16 [16, 32, 64], P(('gr', 'sp'), 'tp')
All inputs are finite; a program needn't handle non-finite values.
Results may differ from a plain program's by a relative error of at most 0.0081.
Values may be sent and summed in bfloat16 or wider, within the bound.
A program may use at most 64 MiB of HBM per device.

v0:
```python
import jax
import jax.numpy as jnp
from jax import lax
from jax.sharding import PartitionSpec as P

HEAD_DIM = 64


def local(mixer_input, key_weight, content_projection_matrix, new_queries, head_stick_offset):
    group_seqs, block_rows, model_width = mixer_input.shape
    key_heads = key_weight.shape[1] // HEAD_DIM
    head_devices = lax.axis_size("tp")
    copies = max(1, head_devices // key_heads)
    input_rows = mixer_input.reshape(group_seqs * block_rows, model_width)
    key_sum = jnp.dot(
        input_rows,
        lax.all_gather(key_weight, "tp", axis=0, tiled=True),
        preferred_element_type=jnp.float32,
    )
    value_sum = jnp.dot(
        input_rows,
        lax.all_gather(content_projection_matrix, "tp", axis=0, tiled=True),
        preferred_element_type=jnp.float32,
    )
    key_rows = key_sum.astype(jnp.bfloat16).reshape(group_seqs, block_rows, key_heads, HEAD_DIM)
    value_rows = value_sum.astype(jnp.bfloat16).reshape(group_seqs, block_rows, key_heads, HEAD_DIM)
    stacked = jnp.concatenate([key_rows, value_rows], axis=3).transpose(0, 2, 1, 3)
    spread = jnp.repeat(stacked, copies, axis=1)
    spread = lax.all_to_all(spread, "tp", split_axis=1, concat_axis=0, tiled=True)
    kv_cache = lax.all_to_all(spread, "sp", split_axis=0, concat_axis=2, tiled=True)
    seq_local = kv_cache.shape[0]
    slot_local = kv_cache.shape[1]
    head_local = new_queries.shape[1]
    inverse_root = HEAD_DIM ** (-0.5)
    offset_values = lax.dynamic_slice_in_dim(
        head_stick_offset, lax.axis_index("tp") * head_local, head_local
    )
    grouped = new_queries.reshape(seq_local, slot_local, head_local // slot_local, HEAD_DIM)
    cache_keys = kv_cache[:, :, :, :HEAD_DIM]
    cache_values = kv_cache[:, :, :, HEAD_DIM:]
    logit_scores = (
        jnp.einsum("bhgd,bhsd->bhgs", grouped, cache_keys, preferred_element_type=jnp.float32)
        * inverse_root
    )
    logit_scores = logit_scores + offset_values.reshape(1, slot_local, -1, 1)
    stay_terms = jax.nn.log_sigmoid(-logit_scores)
    later_terms = lax.cumsum(stay_terms, axis=3, reverse=True) - stay_terms
    weights = jnp.exp(jax.nn.log_sigmoid(logit_scores) + later_terms).astype(jnp.bfloat16)
    result = jnp.einsum(
        "bhgs,bhsd->bhgd", weights, cache_values, preferred_element_type=jnp.float32
    )
    initial_attended_output = result.reshape(seq_local, head_local, HEAD_DIM).astype(jnp.bfloat16)
    return (kv_cache, initial_attended_output)


def solution(mesh):
    return jax.shard_map(
        local,
        mesh=mesh,
        in_specs=(
            P(("gr", "tp"), "sp", None),
            P("tp", None),
            P("tp", None),
            P(("gr", "sp"), "tp", None),
            P(),
        ),
        out_specs=(P(("gr", "sp"), "tp", None, None), P(("gr", "sp"), "tp", None)),
        check_vma=False,
    )
```

profile of v0, /device:TPU:0, one launch (start us, length us, event | category | flops | bytes accessed | tf_op | source)
XLA Modules:
  0.0 139.1 jit_solution(8693301563375391553)
XLA Ops:
  7.2 0.0 copy-start
  7.2 0.0 all-gather.5.cloned.1.call-start
  7.2 0.7 all-gather.5.cloned.1.call-update
  7.9 0.0 all-gather.3.cloned.1.call-start
  8.0 0.7 all-gather.3.cloned.1.call-update
  8.7 24.9 %all-gather.5.cloned.1.call-done = bf16[2048,256]{1,0:T(8,128)(2,1)} async-done(((bf16[1024,256]{1,0:T(8,128)(2,1)}), bf16[2048,256]{1,0:T(8,128)(2,1)}) %all-gather.5.cloned.1.call-update) | async-done | bytes 1048592 | tf_op jit(solution)/shard_map/all_gather | solution.py:22
  33.6 0.0 copy-done
  33.6 3.0 %convolution_convert_fusion = bf16[768,256]{1,0:T(8,128)(2,1)} fusion(bf16[768,2048]{1,0:T(8,128)(2,1)S(1)} %bitcast.47, bf16[2048,256]{1,0:T(8,128)(2,1)} %all-gather.5.cloned.1.call-done), kind=kOutput, calls=%fused_computation.3 | convolution fusion | flops 805502976 | bytes 4587520 | tf_op jit(solution)/shard_map/dot_general | solution.py:20
  36.5 1.2 copy.28
  37.7 1.3 reshape.94
  39.0 17.5 %all-gather.3.cloned.1.call-done = bf16[2048,256]{1,0:T(8,128)(2,1)} async-done(((bf16[1024,256]{1,0:T(8,128)(2,1)}), bf16[2048,256]{1,0:T(8,128)(2,1)}) %all-gather.3.cloned.1.call-update) | async-done | bytes 1048592 | tf_op jit(solution)/shard_map/all_gather | solution.py:17
  56.4 3.0 %convolution_convert_fusion.1 = bf16[768,256]{1,0:T(8,128)(2,1)} fusion(bf16[768,2048]{1,0:T(8,128)(2,1)S(1)} %bitcast.46, bf16[2048,256]{1,0:T(8,128)(2,1)} %all-gather.3.cloned.1.call-done), kind=kOutput, calls=%fused_computation.4 | convolution fusion | flops 805502976 | bytes 4587520 | tf_op jit(solution)/shard_map/dot_general | solution.py:15
  59.4 1.2 copy.27
  60.6 1.3 reshape.93
  61.8 2.9 %maximum_bitcast_fusion = bf16[4,4,192,128]{2,0,3,1:T(4,128)(2,1)} fusion(bf16[4,192,4,64]{1,0,3,2:T(4,128)(2,1)} %reshape.94, bf16[4,192,4,64]{1,0,3,2:T(4,128)(2,1)} %reshape.93), kind=kLoop, calls=%fused_computation.7 | loop fusion | flops 393216 | bytes 1572864 | tf_op jit(solution)/shard_map/transpose | solution.py:27
  64.8 0.0 copy-start.3
  64.8 2.3 %copy.29 = bf16[4,4,192,128]{3,2,0,1:T(8,128)(2,1)} copy(bf16[4,4,192,128]{2,0,3,1:T(4,128)(2,1)} %maximum_bitcast_fusion) | data formatting | bytes 1572864 | tf_op jit(solution)/shard_map/transpose | solution.py:27
  67.1 0.0 copy-start.2
  67.1 14.5 %all_to_all.36 = bf16[4,4,192,128]{3,2,0,1:T(8,128)(2,1)S(1)} all-to-all(bf16[4,4,192,128]{3,2,0,1:T(8,128)(2,1)} %copy.29), channel_id=1, replica_groups=mesh['gr'=2,'sp'=8,'tp'=2] {'tp'}, dimensions={1} | all-to-all | bytes 1572864 | tf_op jit(solution)/shard_map/all_to_all | solution.py:29
  81.6 0.9 copy.31
  82.6 5.5 %all-to-all-start.1 = ((bf16[8,2,192,128]{3,2,1,0:T(8,128)(2,1)}), bf16[8,2,192,128]{3,2,1,0:T(8,128)(2,1)}, u32[]{:S(2)}, u32[]{:S(2)}) async-start(bf16[8,2,192,128]{3,2,1,0:T(8,128)(2,1)} %bitcast.48), calls=%async_computation.1 | async-start | bytes 1572864 | tf_op jit(solution)/shard_map/all_to_all | solution.py:30
  88.1 0.0 copy-done.3
  88.1 0.1 dynamic_slice.3
  88.2 0.1 add.32
  88.3 19.2 %all-to-all-done.1 = bf16[8,2,192,128]{3,2,1,0:T(8,128)(2,1)} async-done(((bf16[8,2,192,128]{3,2,1,0:T(8,128)(2,1)}), bf16[8,2,192,128]{3,2,1,0:T(8,128)(2,1)}, u32[]{:S(2)}, u32[]{:S(2)}) %all-to-all-start.1) | async-done | bytes 786464 | tf_op jit(solution)/shard_map/all_to_all | solution.py:30
  107.4 1.2 copy.32
  108.6 0.0 copy-start.1
  108.6 0.0 copy-done.2
  108.6 0.3 fusion.1
  108.9 0.1 fusion.13
  109.0 0.5 copy-done.1
  109.5 19.9 %reduce-window.6 = f32[1,2,8,12,128]{4,3,2,1,0:T(8,128)S(1)} reduce-window(f32[1,2,8,12,128]{4,3,2,1,0:T(8,128)S(1)} %copy.34, f32[]{:T(128)} %constant.18.clone.1), window={size=1x1x1x1x128 pad=0_0x0_0x0_0x0_0x0_127}, to_apply=%region_0.1 | reduce-window | flops 3121152 | bytes 196612 | tf_op jit(solution)/shard_map/reduce-window
  129.4 0.1 slice_reduce_fusion
  129.5 0.3 reduce-window.9
  129.9 0.1 slice_bitcast_fusion.4
  129.9 0.1 copy.35
  130.0 2.2 %fusion.2 = bf16[1,16,64]{2,1,0:T(8,128)(2,1)} fusion(bf16[1,2,1536,128]{3,2,1,0:T(8,128)(2,1)} %bitcast.51, f32[2,8,1536]{2,1,0:T(8,128)S(1)} %reshape.98, f32[2,8,1536]{2,1,0:T(8,128)S(1)} %fusion.1, f32[2,8,12]{1,2,0:T(8,128)S(1)} %copy.35), kind=kOutput, calls=%fused_computation.6 | convolution fusion | flops 3613696 | bytes 985856 | tf_op jit(solution)/shard_map/bhgs,bhsd->bhgd/dot_general | solution.py:49
  (2 shorter events, 0.0 us)
Async XLA Ops:
  7.2 26.4 %copy-start = (bf16[4,192,2048]{2,1,0:T(8,128)(2,1)S(1)}, bf16[4,192,2048]{2,1,0:T(8,128)(2,1)}, u32[]{:S(2)}) copy-start(bf16[4,192,2048]{2,1,0:T(8,128)(2,1)} %param.5) | copy-start | bytes 9437188
  7.2 26.4 %all-gather.5.cloned.1.call-start = ((), (), s32[]{:S(2)}) async-start(), calls=%async_computation.3 | async-start | bytes 1572864 | tf_op jit(solution)/shard_map/all_gather | solution.py:22
  7.9 48.5 %all-gather.3.cloned.1.call-start = ((), (), s32[]{:S(2)}) async-start(), calls=%async_computation.2 | async-start | bytes 1572864 | tf_op jit(solution)/shard_map/all_gather | solution.py:17
  64.8 23.3 %copy-start.3 = (f32[32]{0:T(128)S(1)}, f32[32]{0:T(128)}, u32[]{:S(2)}) copy-start(f32[32]{0:T(128)} %param.9) | copy-start | bytes 388
  67.1 41.5 %copy-start.2 = (bf16[1,16,64]{2,1,0:T(8,128)(2,1)S(1)}, bf16[1,16,64]{2,1,0:T(8,128)(2,1)}, u32[]{:S(2)}) copy-start(bf16[1,16,64]{2,1,0:T(8,128)(2,1)} %param.8) | copy-start | bytes 6148
  82.6 24.8 %all-to-all-start.1 = ((bf16[8,2,192,128]{3,2,1,0:T(8,128)(2,1)}), bf16[8,2,192,128]{3,2,1,0:T(8,128)(2,1)}, u32[]{:S(2)}, u32[]{:S(2)}) async-start(bf16[8,2,192,128]{3,2,1,0:T(8,128)(2,1)} %bitcast.48), calls=%async_computation.1 | async-start | bytes 1572864 | tf_op jit(solution)/shard_map/all_to_all | solution.py:30
  108.6 0.9 copy-start.1
Sparse Core Ops, SparseCore 0:
  9.5 23.9 all-gather.4
  35.1 21.2 all-gather.2
where the time goes:
time: 140 us; the launch traced here: 139 us
  waiting for transfers between devices  62.9 us (45%)
  other arithmetic  23.2 us (17%)
  blocking collectives  14.5 us (10%)
  between operations  14.1 us (10%)
  local copies, waits for them, and re-layouts  10.3 us (7%)
  matrix products  8.45 us (6%)
  starting transfers between devices  5.59 us (4%)
    all_gather x1, waiting for transfers between devices, local(): lax.all_gather(content_projection_matrix, 'tp', axis=0, tiled=True)  24.9 us
    another operation x2, other arithmetic  20.2 us
    all_to_all x1, waiting for transfers between devices, local(): lax.all_to_all(spread, 'sp', split_axis=0, concat_axis=2, tiled=True)  19.2 us
    all_gather x1, waiting for transfers between devices, local(): lax.all_gather(key_weight, 'tp', axis=0, tiled=True)  17.5 us
    all_to_all x1, blocking collectives, local(): lax.all_to_all(spread, 'tp', split_axis=1, concat_axis=0, tiled=True)  14.5 us
    all_to_all x1, starting transfers between devices, local(): lax.all_to_all(spread, 'sp', split_axis=0, concat_axis=2, tiled=True)  5.52 us
    dot_general x1, matrix products, local(): jnp.dot(input_rows, lax.all_gather(key_weight, 'tp', axis=0, tiled=True),...  2.96 us
    dot_general x1, matrix products, local(): jnp.dot(input_rows, lax.all_gather(content_projection_matrix, 'tp', axis=...  2.95 us
  transfers between devices with their start and end apart: 3, of which 3 were waited for; matrix products, arithmetic and copies ran while one was open for 4% of the time, Pallas kernels for 0%

commit v1 on v0

--- a/solution.py
+++ b/solution.py
@@ -19,7 +19,12 @@
     )
     value_sum = jnp.dot(
         input_rows,
-        lax.all_gather(content_projection_matrix, "tp", axis=0, tiled=True),
+        jnp.concatenate(
+            lax.all_to_all(
+                jnp.stack([content_projection_matrix] * lax.axis_size("tp")), "tp", 0, 0
+            ),
+            axis=0,
+        ),
         preferred_element_type=jnp.float32,
     )
     key_rows = key_sum.astype(jnp.bfloat16).reshape(group_seqs, block_rows, key_heads, HEAD_DIM)

time: 140 us -> 123 us (0.88)
  waiting for transfers between devices: 62.9 us -> 22.9 us
  blocking collectives: 14.5 us -> 38.8 us
  matrix products: 8.45 us -> 6.58 us
  other arithmetic: 23.2 us -> 24.7 us
    all_gather x1 -> x0, waiting for transfers between devices: 24.9 us -> none  [local(): lax.all_gather(content_projection_matrix, 'tp', axis=0, tiled=True)]
    all_to_all x0 -> x1, blocking collectives: none -> 23.9 us  [local(): lax.all_to_all(jnp.stack([content_projection_matrix] * lax.axis_size('tp'...]
    all_gather x1, waiting for transfers between devices: 17.5 us -> 2.81 us  [local(): lax.all_gather(key_weight, 'tp', axis=0, tiled=True)]
    dot_general x1, matrix products: 2.95 us -> 1.08 us  [local(): jnp.dot(input_rows, jnp.concatenate(lax.all_to_all(jnp.stack([content_pro...]
    another operation x2 -> x3, other arithmetic: 20.2 us -> 21.7 us
  transfers between devices with their start and end apart: 3 -> 2, of which waited for: 3 -> 2; matrix products, arithmetic and copies ran while one was open for 4% -> 3% of each run, Pallas kernels for 0% -> 0%
where the time goes in v1:
time: 123 us; the launch traced here: 122 us
  blocking collectives  38.8 us (32%)
  other arithmetic  24.7 us (20%)
  waiting for transfers between devices  22.9 us (19%)
  between operations  14.1 us (11%)
  local copies, waits for them, and re-layouts  9.13 us (7%)
  matrix products  6.58 us (5%)
  starting transfers between devices  6.05 us (5%)
    all_to_all x1, blocking collectives, local(): lax.all_to_all(jnp.stack([content_projection_matrix] * lax.axis_size('tp'...  23.9 us
    another operation x2, other arithmetic  20.2 us
    all_to_all x1, waiting for transfers between devices, local(): lax.all_to_all(spread, 'sp', split_axis=0, concat_axis=2, tiled=True)  19.4 us
    all_to_all x1, blocking collectives, local(): lax.all_to_all(spread, 'tp', split_axis=1, concat_axis=0, tiled=True)  14.8 us
    all_to_all x1, starting transfers between devices, local(): lax.all_to_all(spread, 'sp', split_axis=0, concat_axis=2, tiled=True)  6.02 us
    dot_general x1, matrix products, local(): jnp.dot(input_rows, lax.all_gather(key_weight, 'tp', axis=0, tiled=True),...  2.97 us
    transpose x1, other arithmetic, local(): jnp.concatenate([key_rows, value_rows], axis=3).transpose(0, 2, 1, 3)  2.93 us
    all_gather x1, waiting for transfers between devices, local(): lax.all_gather(key_weight, 'tp', axis=0, tiled=True)  2.81 us
  transfers between devices with their start and end apart: 2, of which 2 were waited for; matrix products, arithmetic and copies ran while one was open for 3% of the time, Pallas kernels for 0%

profile of v1, /device:TPU:0, one launch (start us, length us, event | category | flops | bytes accessed | tf_op | source)
XLA Modules:
  0.0 122.3 jit_solution(17469100163868614885)
XLA Ops:
  7.2 0.0 copy-start
  7.2 0.0 all-gather.2.cloned.1.call-start
  7.2 0.7 all-gather.2.cloned.1.call-update
  7.9 1.5 %pad_maximum_fusion = bf16[2,1024,256]{2,1,0:T(8,128)(2,1)S(1)} fusion(bf16[1,1024,256]{2,1,0:T(8,128)(2,1)} %bitcast.58), kind=kLoop, calls=%fused_computation.8 | loop fusion | flops 524288 | bytes 1572864 | tf_op jit(solution)/shard_map/stack | solution.py:24
  9.4 23.9 %all_to_all.41 = bf16[2,1024,256]{2,1,0:T(8,128)(2,1)S(1)} all-to-all(bf16[2,1024,256]{2,1,0:T(8,128)(2,1)S(1)} %pad_maximum_fusion), channel_id=1, replica_groups=mesh['gr'=2,'sp'=8,'tp'=2] {'tp'}, dimensions={0} | all-to-all | bytes 2097152 | tf_op jit(solution)/shard_map/all_to_all | solution.py:23
  33.4 0.0 copy-done
  33.4 1.1 fusion.2
  34.5 1.3 %reshape.98 = bf16[4,192,4,64]{1,0,3,2:T(4,128)(2,1)} reshape(bf16[768,256]{0,1:T(8,128)(2,1)S(1)} %fusion.2) | data formatting | bytes 786432 | tf_op jit(solution)/shard_map/reshape | solution.py:31
  35.7 2.8 %all-gather.2.cloned.1.call-done = bf16[2048,256]{1,0:T(8,128)(2,1)} async-done(((bf16[1024,256]{1,0:T(8,128)(2,1)}), bf16[2048,256]{1,0:T(8,128)(2,1)}) %all-gather.2.cloned.1.call-update) | async-done | bytes 1048592 | tf_op jit(solution)/shard_map/all_gather | solution.py:17
  38.5 3.0 %convolution_convert_fusion.1 = bf16[768,256]{1,0:T(8,128)(2,1)} fusion(bf16[768,2048]{1,0:T(8,128)(2,1)S(1)} %bitcast.50, bf16[2048,256]{1,0:T(8,128)(2,1)} %all-gather.2.cloned.1.call-done), kind=kOutput, calls=%fused_computation.4 | convolution fusion | flops 805502976 | bytes 4587520 | tf_op jit(solution)/shard_map/dot_general | solution.py:15
  41.5 1.2 copy.26
  42.7 1.3 %reshape.96 = bf16[4,192,4,64]{1,0,3,2:T(4,128)(2,1)} reshape(bf16[768,256]{0,1:T(8,128)(2,1)S(1)} %copy.26) | data formatting | bytes 786432 | tf_op jit(solution)/shard_map/reshape | solution.py:30
  44.0 2.9 %maximum_bitcast_fusion = bf16[4,4,192,128]{2,0,3,1:T(4,128)(2,1)} fusion(bf16[4,192,4,64]{1,0,3,2:T(4,128)(2,1)} %reshape.98, bf16[4,192,4,64]{1,0,3,2:T(4,128)(2,1)} %reshape.96), kind=kLoop, calls=%fused_computation.9 | loop fusion | flops 393216 | bytes 1572864 | tf_op jit(solution)/shard_map/transpose | solution.py:32
  46.9 0.0 copy-start.3
  46.9 2.3 %copy.27 = bf16[4,4,192,128]{3,2,0,1:T(8,128)(2,1)} copy(bf16[4,4,192,128]{2,0,3,1:T(4,128)(2,1)} %maximum_bitcast_fusion) | data formatting | bytes 1572864 | tf_op jit(solution)/shard_map/transpose | solution.py:32
  49.2 0.0 copy-start.2
  49.2 14.8 %all_to_all.42 = bf16[4,4,192,128]{3,2,0,1:T(8,128)(2,1)S(1)} all-to-all(bf16[4,4,192,128]{3,2,0,1:T(8,128)(2,1)} %copy.27), channel_id=1, replica_groups=mesh['gr'=2,'sp'=8,'tp'=2] {'tp'}, dimensions={1} | all-to-all | bytes 1572864 | tf_op jit(solution)/shard_map/all_to_all | solution.py:34
  64.1 0.9 copy.29
  65.0 6.0 %all-to-all-start.2 = ((bf16[8,2,192,128]{3,2,1,0:T(8,128)(2,1)}), bf16[8,2,192,128]{3,2,1,0:T(8,128)(2,1)}, u32[]{:S(2)}, u32[]{:S(2)}) async-start(bf16[8,2,192,128]{3,2,1,0:T(8,128)(2,1)} %bitcast.52), calls=%async_computation.2 | async-start | bytes 1572864 | tf_op jit(solution)/shard_map/all_to_all | solution.py:35
  71.0 0.0 copy-done.3
  71.0 0.1 dynamic_slice.3
  71.1 0.1 add.32
  71.2 19.4 %all-to-all-done.2 = bf16[8,2,192,128]{3,2,1,0:T(8,128)(2,1)} async-done(((bf16[8,2,192,128]{3,2,1,0:T(8,128)(2,1)}), bf16[8,2,192,128]{3,2,1,0:T(8,128)(2,1)}, u32[]{:S(2)}, u32[]{:S(2)}) %all-to-all-start.2) | async-done | bytes 786464 | tf_op jit(solution)/shard_map/all_to_all | solution.py:35
  90.6 1.2 copy.30
  91.8 0.0 copy-start.1
  91.8 0.0 copy-done.2
  91.8 0.3 fusion.1
  92.1 0.1 fusion.14
  92.2 0.5 copy-done.1
  92.7 19.9 %reduce-window.6 = f32[1,2,8,12,128]{4,3,2,1,0:T(8,128)S(1)} reduce-window(f32[1,2,8,12,128]{4,3,2,1,0:T(8,128)S(1)} %copy.32, f32[]{:T(128)} %constant.18.clone.1), window={size=1x1x1x1x128 pad=0_0x0_0x0_0x0_0x0_127}, to_apply=%region_0.1 | reduce-window | flops 3121152 | bytes 196612 | tf_op jit(solution)/shard_map/reduce-window
  112.6 0.1 slice_reduce_fusion
  112.7 0.3 reduce-window.9
  113.1 0.1 slice_bitcast_fusion.4
  113.1 0.1 copy.33
  113.2 2.2 %fusion.3 = bf16[1,16,64]{2,1,0:T(8,128)(2,1)} fusion(bf16[1,2,1536,128]{3,2,1,0:T(8,128)(2,1)} %bitcast.56, f32[2,8,1536]{2,1,0:T(8,128)S(1)} %reshape.102, f32[2,8,1536]{2,1,0:T(8,128)S(1)} %fusion.1, f32[2,8,12]{1,2,0:T(8,128)S(1)} %copy.33), kind=kOutput, calls=%fused_computation.7 | convolution fusion | flops 3613696 | bytes 985856 | tf_op jit(solution)/shard_map/bhgs,bhsd->bhgd/dot_general | solution.py:54
  (2 shorter events, 0.0 us)
Async XLA Ops:
  7.2 26.2 %copy-start = (bf16[4,192,2048]{2,1,0:T(8,128)(2,1)S(1)}, bf16[4,192,2048]{2,1,0:T(8,128)(2,1)}, u32[]{:S(2)}) copy-start(bf16[4,192,2048]{2,1,0:T(8,128)(2,1)} %param.5) | copy-start | bytes 9437188
  7.2 31.3 %all-gather.2.cloned.1.call-start = ((), (), s32[]{:S(2)}) async-start(), calls=%async_computation.3 | async-start | bytes 1572864 | tf_op jit(solution)/shard_map/all_gather | solution.py:17
  46.9 24.1 %copy-start.3 = (f32[32]{0:T(128)S(1)}, f32[32]{0:T(128)}, u32[]{:S(2)}) copy-start(f32[32]{0:T(128)} %param.9) | copy-start | bytes 388
  49.2 42.6 %copy-start.2 = (bf16[1,16,64]{2,1,0:T(8,128)(2,1)S(1)}, bf16[1,16,64]{2,1,0:T(8,128)(2,1)}, u32[]{:S(2)}) copy-start(bf16[1,16,64]{2,1,0:T(8,128)(2,1)} %param.8) | copy-start | bytes 6148
  65.0 25.6 %all-to-all-start.2 = ((bf16[8,2,192,128]{3,2,1,0:T(8,128)(2,1)}), bf16[8,2,192,128]{3,2,1,0:T(8,128)(2,1)}, u32[]{:S(2)}, u32[]{:S(2)}) async-start(bf16[8,2,192,128]{3,2,1,0:T(8,128)(2,1)} %bitcast.52), calls=%async_computation.2 | async-start | bytes 1572864 | tf_op jit(solution)/shard_map/all_to_all | solution.py:35
  91.8 0.9 copy-start.1
Sparse Core Ops, SparseCore 0:
  9.5 28.9 all-gather.1
